TPU v7x, 32 devices: a whole 2x2x4 slice. The times are simulated.
32 devices in a mesh: fs: 4 (over y, x), tp: 8 (over z, core).
Axes of the slice: x: 2, y: 2, z: 4, core: 2. Of those that a mesh axis runs over, the one named last changes fastest.
Arguments:
- hidden_in: bfloat16 [6144, 4096], P('fs', 'tp'), may hold values from -6 to 6
- forget_pre: bfloat16 [6144, 2048], P('fs', 'tp'), may hold values from -8 to 8
- forget_cot: bfloat16 [6144, 2048], P('fs', 'tp'), may hold values from -0.4375 to 0.4375
- lower_bound: float32 [2048], P('tp'), may hold values from 0.05 to 0.9
- head_out: bfloat16 [6144, 2048], P('fs', 'tp'), may hold values from -6 to 6
- out_cot: bfloat16 [6144, 4096], P('fs', 'tp'), may hold values from -0.109375 to 0.109375
- basis_forget: bfloat16 [2048, 256], replicated, may hold values from -0.37565048 to 0.37565048
- basis_output: bfloat16 [2048, 256], replicated, may hold values from -0.37565048 to 0.37565048
- weight_forget: float32 [2048, 4096], P('fs', 'tp'), may hold values from -0.09375 to 0.09375
- weight_output: float32 [4096, 2048], P('tp', 'fs'), may hold values from -0.125 to 0.125
- mean_forget: float32 [256, 4096], P('fs', 'tp'), may hold values from -3.5 to 3.5
- var_forget: float32 [256, 4096], P('fs', 'tp'), may hold values from 0.003 to 0.05
- mean_output: float32 [256, 4096], P('fs', 'tp'), may hold values from -3.5 to 3.5
- var_output: float32 [256, 4096], P('fs', 'tp'), may hold values from 0.003 to 0.05
Outputs:
- step_forget: float32 [2048, 4096], P('fs', 'tp')
- step_output: float32 [4096, 2048], P('tp', 'fs')
- new_forget: float32 [2048, 4096], P('fs', 'tp')
- new_output: float32 [4096, 2048], P('tp', 'fs')
- mean_forget_new: float32 [256, 4096], P('fs', 'tp')
- var_forget_new: float32 [256, 4096], P('fs', 'tp')
- mean_output_new: float32 [256, 4096], P('fs', 'tp')
- var_output_new: float32 [256, 4096], P('fs', 'tp')
- copy_forget: bfloat16 [2048, 4096], P(None, 'tp')
- copy_output: bfloat16 [4096, 2048], P('tp')
All inputs are finite; a program needn't handle non-finite values.
Results may differ from a plain program's by a relative error of at most 0.014.
Values may be sent and summed in bfloat16 or wider, within the bound.
A program may use at most 64 MiB of HBM per device.

v0:
```python
import jax
import jax.numpy as jnp
from jax import lax
from jax.sharding import PartitionSpec as P

D = 4096
HW = 2048
beta_one = 0.9
beta_two = 0.99
adam_eps = 1e-08
norm_eps = 1e-06
step_rate = 0.02


def moment_update(mean, var, proj):
    mean_new = beta_one * mean + (1.0 - beta_one) * proj
    var_new = beta_two * var + (1.0 - beta_two) * proj * proj
    return (mean_new, var_new, mean_new / (jnp.sqrt(var_new) + adam_eps))


def split_product(coords, tokens_data):
    upper = coords.astype(jnp.bfloat16)
    lower = (coords - upper.astype(jnp.float32)).astype(jnp.bfloat16)
    first = jnp.einsum("tr,td->rd", upper, tokens_data, preferred_element_type=jnp.float32)
    second = jnp.einsum("tr,td->rd", lower, tokens_data, preferred_element_type=jnp.float32)
    return first + second


def per_device(
    hidden_in,
    forget_pre,
    forget_cot,
    lower_bound,
    head_out,
    out_cot,
    basis_forget,
    basis_output,
    weight_forget,
    weight_output,
    mean_forget,
    var_forget,
    mean_output,
    var_output,
):
    highest = lax.Precision.HIGHEST
    fs_rank = lax.axis_index("fs")
    tp_rank = lax.axis_index("tp")
    unit_count = forget_pre.shape[1]
    feat_cols = hidden_in.shape[1]
    head_rows = weight_forget.shape[0]
    sigmoid_z = jax.nn.sigmoid(forget_pre.astype(jnp.float32))
    keep_rate = 1.0 - lower_bound
    forget_val = lower_bound + keep_rate * sigmoid_z
    gate_grad = (
        forget_cot.astype(jnp.float32) * keep_rate * sigmoid_z * (1.0 - sigmoid_z) / forget_val
    ).astype(jnp.bfloat16)
    rows_forget = lax.dynamic_slice_in_dim(basis_forget, fs_rank * head_rows, head_rows, 0).astype(
        jnp.float32
    )
    rows_output = lax.dynamic_slice_in_dim(basis_output, fs_rank * head_rows, head_rows, 0).astype(
        jnp.float32
    )
    local_forget = lax.dynamic_slice_in_dim(basis_forget, tp_rank * unit_count, unit_count, 0)
    local_output = lax.dynamic_slice_in_dim(basis_output, tp_rank * unit_count, unit_count, 0)
    coords_forget = jnp.dot(gate_grad, local_forget, preferred_element_type=jnp.float32)
    coords_output = jnp.dot(head_out, local_output, preferred_element_type=jnp.float32)
    coords_forget, coords_output = lax.psum((coords_forget, coords_output), "tp")
    part_forget = split_product(coords_forget, hidden_in)
    part_output = split_product(coords_output, out_cot)
    proj = lax.psum_scatter(
        jnp.concatenate([part_forget, part_output], axis=1), "fs", scatter_dimension=0, tiled=True
    )
    mean_f, var_f, dir_forget = moment_update(mean_forget, var_forget, proj[:, :feat_cols])
    mean_o, var_o, dir_output = moment_update(mean_output, var_output, proj[:, feat_cols:])
    dir_forget, dir_output = (
        lax.all_gather(dir_forget, "fs", axis=0, tiled=True),
        lax.all_gather(dir_output, "fs", axis=0, tiled=True),
    )
    upd_forget = jnp.dot(rows_forget, dir_forget, precision=highest)
    upd_output = jnp.dot(rows_output, dir_output, precision=highest)
    total = float(HW * D)
    sum_forget, sum_output = lax.psum(
        (jnp.sum(upd_forget * upd_forget), jnp.sum(upd_output * upd_output)), ("fs", "tp")
    )
    step_forget = upd_forget * lax.rsqrt(sum_forget / total + norm_eps)
    step_output = (upd_output * lax.rsqrt(sum_output / total + norm_eps)).T
    new_forget = weight_forget - step_rate * step_forget
    new_output = weight_output - step_rate * step_output
    copy_forget, copy_output = (
        lax.all_gather(new_forget.astype(jnp.bfloat16), "fs", axis=0, tiled=True),
        lax.all_gather(new_output.astype(jnp.bfloat16), "fs", axis=1, tiled=True),
    )
    return (
        step_forget,
        step_output,
        new_forget,
        new_output,
        mean_f,
        var_f,
        mean_o,
        var_o,
        copy_forget,
        copy_output,
    )


def solution(mesh):
    return jax.shard_map(
        per_device,
        mesh=mesh,
        in_specs=(
            P("fs", "tp"),
            P("fs", "tp"),
            P("fs", "tp"),
            P("tp"),
            P("fs", "tp"),
            P("fs", "tp"),
            P(),
            P(),
            P("fs", "tp"),
            P("tp", "fs"),
            P("fs", "tp"),
            P("fs", "tp"),
            P("fs", "tp"),
            P("fs", "tp"),
        ),
        out_specs=(
            P("fs", "tp"),
            P("tp", "fs"),
            P("fs", "tp"),
            P("tp", "fs"),
            P("fs", "tp"),
            P("fs", "tp"),
            P("fs", "tp"),
            P("fs", "tp"),
            P(None, "tp"),
            P("tp", None),
        ),
        check_vma=False,
    )
```

profile of v0, /device:TPU:0, one launch (start us, length us, event | category | flops | bytes accessed | tf_op | source)
XLA Modules:
  0.0 282.4 jit_solution(18277025858053126377)
XLA Ops:
  7.2 0.0 all-reduce.4.cloned.1.call-start
  7.3 0.8 broadcast_subtract_fusion
  8.1 2.8 convolution_bitcast_fusion
  10.9 3.0 %fusion = f32[1536,256]{1,0:T(8,128)} fusion(bf16[1536,256]{1,0:T(8,128)(2,1)S(1)} %copy-done.10, bf16[1536,256]{1,0:T(8,128)(2,1)S(1)} %copy-done.11, f32[256]{0:T(256)S(1)} %copy-done.9, f32[256]{0:T(256)S(1)} %broadcast_subtract_fusion, bf16[2048,256]{1,0:T(8,128)(2,1)} %param.20, s32[]{:T(128)S(6)} %select_n.9), kind=kOutput, calls=%fused_computation.12 | convolution fusion | flops 206438400 | bytes 3278852 | tf_op jit(solution)/shard_map/dot_general | solution.py:65
  13.9 0.0 all-reduce.4.cloned.1.call-update
  13.9 0.0 reduce-scatter.2.cloned.1.call-start
  13.9 79.7 %all-reduce.4.cloned.1.call-done = (f32[1536,256]{0,1:T(8,128)}, f32[1536,256]{1,0:T(8,128)}) async-done(((f32[1536,256]{0,1:T(8,128)}, f32[1536,256]{1,0:T(8,128)}), (f32[1536,256]{0,1:T(8,128)}, f32[1536,256]{1,0:T(8,128)})) %all-reduce.4.cloned.1.call-update) | async-done | bytes 3145744 | tf_op jit(solution)/shard_map/psum | solution.py:67
  93.7 2.1 fusion.2
  95.8 0.6 convolution_add_fusion
  96.4 0.8 copy-done.1
  97.2 0.5 copy-done.2
  97.7 0.6 fusion.5
  98.3 0.6 convolution_add_fusion.1
  98.9 1.1 pad_maximum_fusion
  100.0 0.0 all-gather.3.cloned.1.call-start
  100.1 28.0 %reduce-scatter.2.cloned.1.call-done = f32[64,1024]{1,0:T(8,128)} async-done(((f32[256,1024]{1,0:T(8,128)}), f32[64,1024]{1,0:T(8,128)}) %reduce-scatter.2.cloned.1.call-update) | async-done | bytes 262160 | tf_op jit(solution)/shard_map/reduce_scatter | solution.py:70
  128.0 1.9 add_divide_fusion
  129.9 10.1 %all_gather.13 = f32[256,512]{1,0:T(8,128)S(1)} all-gather(f32[64,512]{1,0:T(8,128)S(1)} %get-tuple-element.20), channel_id=1, replica_groups=mesh['fs'=4,'tp'=8] {'fs'}, dimensions={0}, use_global_device_ids=true | all-gather | bytes 655360 | tf_op jit(solution)/shard_map/all_gather | solution.py:77
  140.0 9.7 %all_gather.12 = f32[256,512]{1,0:T(8,128)S(1)} all-gather(f32[64,512]{1,0:T(8,128)S(1)} %get-tuple-element.26), channel_id=1, replica_groups=mesh['fs'=4,'tp'=8] {'fs'}, dimensions={0}, use_global_device_ids=true | all-gather | bytes 655360 | tf_op jit(solution)/shard_map/all_gather | solution.py:76
  149.7 2.3 multiply_reduce_fusion.1
  152.0 3.2 %multiply_reduce_fusion = (f32[]{:T(128)}, f32[512,512]{1,0:T(8,128)}) fusion(f32[256,512]{1,0:T(8,128)S(1)} %all_gather.13, bf16[2048,256]{1,0:T(8,128)(2,1)} %param.21, s32[]{:T(128)S(6)} %select_n.8), kind=kOutput, calls=%fused_computation.10 | convolution fusion | flops 805830656 | bytes 1835016 | tf_op jit(solution)/shard_map/dot_general | solution.py:80
  155.1 39.5 %all-reduce = (f32[]{:T(128)}, f32[]{:T(128)}) all-reduce(f32[]{:T(128)} %get-tuple-element.29, f32[]{:T(128)} %get-tuple-element.31), channel_id=1, replica_groups=mesh['fs'=4,'tp'=8] {'fs','tp'}, use_global_device_ids=true, to_apply=%region_4.0 | all-reduce | flops 2 | bytes 16 | tf_op jit(solution)/shard_map/psum | solution.py:82
  195.4 3.1 %fusion.21 = (bf16[512,512]{1,0:T(8,128)(2,1)}, f32[512,512]{1,0:T(8,128)}, f32[512,512]{1,0:T(8,128)}) fusion(f32[512,512]{1,0:T(8,128)} %param.22, f32[512,512]{1,0:T(8,128)S(1)} %get-tuple-element.30, f32[]{:T(128)S(6)} %rsqrt.6), kind=kLoop, calls=%fused_computation.41 | loop fusion | flops 1048576 | bytes 4718596 | tf_op jit(solution)/shard_map/convert_element_type | solution.py:90
  198.4 0.0 all-gather.3.cloned.1.call-update
  198.5 0.0 all-gather.5.cloned.1.call-start
  198.5 1.6 copy.24
  200.8 3.1 %fusion.20 = (bf16[512,512]{1,0:T(8,128)(2,1)}, f32[512,512]{1,0:T(8,128)}, f32[512,512]{1,0:T(8,128)}) fusion(f32[512,512]{1,0:T(8,128)} %param.23, f32[512,512]{0,1:T(8,128)S(1)} %copy.24, f32[]{:T(128)S(6)} %rsqrt.7), kind=kLoop, calls=%fused_computation.40 | loop fusion | flops 1048576 | bytes 4718596 | tf_op jit(solution)/shard_map/convert_element_type | solution.py:91
  203.9 0.0 all-gather.5.cloned.1.call-update
  203.9 30.1 %all-gather.3.cloned.1.call-done = bf16[2048,512]{1,0:T(8,128)(2,1)} async-done(((bf16[512,512]{1,0:T(8,128)(2,1)}), bf16[2048,512]{1,0:T(8,128)(2,1)}) %all-gather.3.cloned.1.call-update) | async-done | bytes 2097168 | tf_op jit(solution)/shard_map/all_gather | solution.py:90
  234.0 37.3 %all-gather.5.cloned.1.call-done = bf16[512,2048]{1,0:T(8,128)(2,1)} async-done(((bf16[512,512]{1,0:T(8,128)(2,1)}), bf16[512,2048]{1,0:T(8,128)(2,1)}) %all-gather.5.cloned.1.call-update) | async-done | bytes 2097168 | tf_op jit(solution)/shard_map/all_gather | solution.py:91
  271.4 3.2 %copy.29 = bf16[2048,512]{1,0:T(8,128)(2,1)} copy(bf16[2048,512]{1,0:T(8,128)(2,1)} %all-gather.3.cloned.1.call-done) | data formatting | bytes 4194304
  274.6 1.3 copy.30
  (23 shorter events, 0.1 us)
Async XLA Ops:
  7.2 86.5 %copy-start = (bf16[1536,512]{1,0:T(8,128)(2,1)S(1)}, bf16[1536,512]{1,0:T(8,128)(2,1)}, u32[]{:S(2)}) copy-start(bf16[1536,512]{1,0:T(8,128)(2,1)} %param.19) | copy-start | bytes 4718596
  7.2 3.7 %copy-start.9 = (f32[256]{0:T(256)S(1)}, f32[256]{0:T(256)}, u32[]{:S(2)}) copy-start(f32[256]{0:T(256)} %param.17) | copy-start | bytes 3076
  7.2 3.7 %copy-start.11 = (bf16[1536,256]{1,0:T(8,128)(2,1)S(1)}, bf16[1536,256]{1,0:T(8,128)(2,1)}, u32[]{:S(2)}) copy-start(bf16[1536,256]{1,0:T(8,128)(2,1)} %param.16) | copy-start | bytes 2359300
  7.2 3.7 %copy-start.10 = (bf16[1536,256]{1,0:T(8,128)(2,1)S(1)}, bf16[1536,256]{1,0:T(8,128)(2,1)}, u32[]{:S(2)}) copy-start(bf16[1536,256]{1,0:T(8,128)(2,1)} %param.15) | copy-start | bytes 2359300
  7.2 86.4 %all-reduce.4.cloned.1.call-start = ((), (), s32[]{:S(2)}) async-start(), calls=%async_computation.4 | async-start | bytes 6291456 | tf_op jit(solution)/shard_map/psum | solution.py:67
  13.9 114.1 %reduce-scatter.2.cloned.1.call-start = ((), (), s32[]{:S(2)}) async-start(), calls=%async_computation.1 | async-start | bytes 1310720 | tf_op jit(solution)/shard_map/reduce_scatter | solution.py:70
  93.7 2.1 copy-start.3
  95.8 1.4 copy-start.1
  95.8 1.9 copy-start.2
  98.9 29.2 %copy-start.5 = (f32[64,512]{1,0:T(8,128)S(1)}, f32[64,512]{1,0:T(8,128)}, u32[]{:S(2)}) copy-start(f32[64,512]{1,0:T(8,128)} %param.27) | copy-start | bytes 393220
  98.9 29.2 %copy-start.6 = (f32[64,512]{1,0:T(8,128)S(1)}, f32[64,512]{1,0:T(8,128)}, u32[]{:S(2)}) copy-start(f32[64,512]{1,0:T(8,128)} %param.26) | copy-start | bytes 393220
  98.9 29.1 %copy-start.7 = (f32[64,512]{1,0:T(8,128)S(1)}, f32[64,512]{1,0:T(8,128)}, u32[]{:S(2)}) copy-start(f32[64,512]{1,0:T(8,128)} %param.25) | copy-start | bytes 393220
  98.9 29.1 %copy-start.8 = (f32[64,512]{1,0:T(8,128)S(1)}, f32[64,512]{1,0:T(8,128)}, u32[]{:S(2)}) copy-start(f32[64,512]{1,0:T(8,128)} %param.24) | copy-start | bytes 393220
  100.0 134.0 %all-gather.3.cloned.1.call-start = ((), (), s32[]{:S(2)}) async-start(), calls=%async_computation.2 | async-start | bytes 2621440 | tf_op jit(solution)/shard_map/all_gather | solution.py:90
  198.5 72.9 %all-gather.5.cloned.1.call-start = ((), (), s32[]{:S(2)}) async-start(), calls=%async_computation.3 | async-start | bytes 2621440 | tf_op jit(solution)/shard_map/all_gather | solution.py:91
  271.4 3.2 %copy-start.4 = (bf16[512,2048]{1,0:T(8,128)(2,1)S(1)}, bf16[512,2048]{1,0:T(8,128)(2,1)}, u32[]{:S(2)}) copy-start(bf16[512,2048]{1,0:T(8,128)(2,1)} %all-gather.5.cloned.1.call-done) | copy-start | bytes 6291460
Sparse Core Ops, SparseCore 0:
  14.0 79.5 all-reduce.3
  100.1 27.8 reduce-scatter.1
  198.6 35.3 all-gather.2
  236.3 35.0 all-gather.4
where the time goes:
time: 283 us; the launch traced here: 282 us
  waiting for transfers between devices  175 us (62%)
  blocking collectives  59.3 us (21%)
  between operations  15.3 us (5%)
  matrix products  15.1 us (5%)
  other arithmetic  9.91 us (4%)
  local copies, waits for them, and re-layouts  7.41 us (3%)
    psum x1, waiting for transfers between devices, per_device(): lax.psum((coords_forget, coords_output), 'tp')  79.7 us
    psum x1, blocking collectives, per_device(): lax.psum((jnp.sum(upd_forget * upd_forget), jnp.sum(upd_output * upd_outp...  39.5 us
    all_gather x1, waiting for transfers between devices, per_device(): lax.all_gather(new_output.astype(jnp.bfloat16), 'fs', axis=1, tiled=True)  37.3 us
    all_gather x1, waiting for transfers between devices, per_device(): lax.all_gather(new_forget.astype(jnp.bfloat16), 'fs', axis=0, tiled=True)  30.1 us
    reduce_scatter x1, waiting for transfers between devices, per_device(): lax.psum_scatter(jnp.concatenate([part_forget, part_output], axis=1), 'fs...  28 us
    all_gather x1, blocking collectives, per_device(): lax.all_gather(dir_output, 'fs', axis=0, tiled=True)  10.1 us
    all_gather x1, blocking collectives, per_device(): lax.all_gather(dir_forget, 'fs', axis=0, tiled=True)  9.67 us
    unnamed x26, local copies, waits for them, and re-layouts  5.86 us
  transfers between devices with their start and end apart: 4, of which 4 were waited for; matrix products, arithmetic and copies ran while one was open for 2% of the time, Pallas kernels for 0%

commit v1 on v0

--- a/solution.py
+++ b/solution.py
@@ -80,7 +80,7 @@
     upd_output = jnp.dot(rows_output, dir_output, precision=highest)
     total = float(HW * D)
     sum_forget, sum_output = lax.psum(
-        (jnp.sum(upd_forget * upd_forget), jnp.sum(upd_output * upd_output)), ("fs", "tp")
+        lax.psum((jnp.sum(upd_forget * upd_forget), jnp.sum(upd_output * upd_output)), "tp"), "fs"
     )
     step_forget = upd_forget * lax.rsqrt(sum_forget / total + norm_eps)
     step_output = (upd_output * lax.rsqrt(sum_output / total + norm_eps)).T

time: 283 us -> 264 us (0.933)
  blocking collectives: 59.3 us -> 43.5 us
  waiting for transfers between devices: 175 us -> 172 us
    psum x1, blocking collectives: 39.5 us -> 14.2 us  [per_device(): lax.psum((jnp.sum(upd_forget * upd_forget), jnp.sum(upd_output * upd_outp...]
    psum x0 -> x1, blocking collectives: none -> 9.53 us  [per_device(): lax.psum(lax.psum((jnp.sum(upd_forget * upd_forget), jnp.sum(upd_output *...]
    all_gather x1, waiting for transfers between devices: 30.1 us -> 26.5 us  [per_device(): lax.all_gather(new_forget.astype(jnp.bfloat16), 'fs', axis=0, tiled=True)]
where the time goes in v1:
time: 264 us; the launch traced here: 263 us
  waiting for transfers between devices  172 us (65%)
  blocking collectives  43.5 us (16%)
  between operations  15.3 us (6%)
  matrix products  15.1 us (6%)
  other arithmetic  9.97 us (4%)
  local copies, waits for them, and re-layouts  7.41 us (3%)
    psum x1, waiting for transfers between devices, per_device(): lax.psum((coords_forget, coords_output), 'tp')  79.7 us
    all_gather x1, waiting for transfers between devices, per_device(): lax.all_gather(new_output.astype(jnp.bfloat16), 'fs', axis=1, tiled=True)  37.3 us
    reduce_scatter x1, waiting for transfers between devices, per_device(): lax.psum_scatter(jnp.concatenate([part_forget, part_output], axis=1), 'fs...  28 us
    all_gather x1, waiting for transfers between devices, per_device(): lax.all_gather(new_forget.astype(jnp.bfloat16), 'fs', axis=0, tiled=True)  26.5 us
    psum x1, blocking collectives, per_device(): lax.psum((jnp.sum(upd_forget * upd_forget), jnp.sum(upd_output * upd_outp...  14.2 us
    all_gather x1, blocking collectives, per_device(): lax.all_gather(dir_output, 'fs', axis=0, tiled=True)  10.1 us
    all_gather x1, blocking collectives, per_device(): lax.all_gather(dir_forget, 'fs', axis=0, tiled=True)  9.67 us
    psum x1, blocking collectives, per_device(): lax.psum(lax.psum((jnp.sum(upd_forget * upd_forget), jnp.sum(upd_output *...  9.53 us
  transfers between devices with their start and end apart: 4, of which 4 were waited for; matrix products, arithmetic and copies ran while one was open for 2% of the time, Pallas kernels for 0%

profile of v1, /device:TPU:0, one launch (start us, length us, event | category | flops | bytes accessed | tf_op | source)
XLA Modules:
  0.0 263.1 jit_solution(5047284948646170643)
XLA Ops:
  7.2 0.0 all-reduce.5.cloned.1.call-start
  7.3 0.8 broadcast_subtract_fusion
  8.1 2.8 %convolution_bitcast_fusion = f32[1536,256]{0,1:T(8,128)} fusion(bf16[1536,256]{1,0:T(8,128)(2,1)} %param.18, bf16[2048,256]{1,0:T(8,128)(2,1)} %param.21, s32[]{:T(128)S(6)} %select_n.9), kind=kOutput, calls=%fused_computation | convolution fusion | flops 201326592 | bytes 2490372 | tf_op jit(solution)/shard_map/dot_general | solution.py:66
  10.9 3.0 %fusion = f32[1536,256]{1,0:T(8,128)} fusion(bf16[1536,256]{1,0:T(8,128)(2,1)S(1)} %copy-done.10, bf16[1536,256]{1,0:T(8,128)(2,1)S(1)} %copy-done.11, f32[256]{0:T(256)S(1)} %copy-done.9, f32[256]{0:T(256)S(1)} %broadcast_subtract_fusion, bf16[2048,256]{1,0:T(8,128)(2,1)} %param.20, s32[]{:T(128)S(6)} %select_n.9), kind=kOutput, calls=%fused_computation.12 | convolution fusion | flops 206438400 | bytes 3278852 | tf_op jit(solution)/shard_map/dot_general | solution.py:65
  13.9 0.0 all-reduce.5.cloned.1.call-update
  13.9 0.0 reduce-scatter.2.cloned.1.call-start
  13.9 79.7 %all-reduce.5.cloned.1.call-done = (f32[1536,256]{0,1:T(8,128)}, f32[1536,256]{1,0:T(8,128)}) async-done(((f32[1536,256]{0,1:T(8,128)}, f32[1536,256]{1,0:T(8,128)}), (f32[1536,256]{0,1:T(8,128)}, f32[1536,256]{1,0:T(8,128)})) %all-reduce.5.cloned.1.call-update) | async-done | bytes 3145744 | tf_op jit(solution)/shard_map/psum | solution.py:67
  93.7 2.1 fusion.2
  95.8 0.6 convolution_add_fusion
  96.4 0.8 copy-done.1
  97.2 0.5 copy-done.2
  97.7 0.6 fusion.5
  98.3 0.6 convolution_add_fusion.1
  98.9 1.1 pad_maximum_fusion
  100.0 0.0 all-gather.3.cloned.1.call-start
  100.1 28.0 %reduce-scatter.2.cloned.1.call-done = f32[64,1024]{1,0:T(8,128)} async-done(((f32[256,1024]{1,0:T(8,128)}), f32[64,1024]{1,0:T(8,128)}) %reduce-scatter.2.cloned.1.call-update) | async-done | bytes 262160 | tf_op jit(solution)/shard_map/reduce_scatter | solution.py:70
  128.0 1.9 add_divide_fusion
  129.9 10.1 %all_gather.13 = f32[256,512]{1,0:T(8,128)S(1)} all-gather(f32[64,512]{1,0:T(8,128)S(1)} %get-tuple-element.22), channel_id=1, replica_groups=mesh['fs'=4,'tp'=8] {'fs'}, dimensions={0}, use_global_device_ids=true | all-gather | bytes 655360 | tf_op jit(solution)/shard_map/all_gather | solution.py:77
  140.0 9.7 %all_gather.12 = f32[256,512]{1,0:T(8,128)S(1)} all-gather(f32[64,512]{1,0:T(8,128)S(1)} %get-tuple-element.28), channel_id=1, replica_groups=mesh['fs'=4,'tp'=8] {'fs'}, dimensions={0}, use_global_device_ids=true | all-gather | bytes 655360 | tf_op jit(solution)/shard_map/all_gather | solution.py:76
  149.7 2.3 multiply_reduce_fusion.1
  152.0 3.2 %multiply_reduce_fusion = (f32[]{:T(128)}, f32[512,512]{1,0:T(8,128)}) fusion(f32[256,512]{1,0:T(8,128)S(1)} %all_gather.13, bf16[2048,256]{1,0:T(8,128)(2,1)} %param.21, s32[]{:T(128)S(6)} %select_n.8), kind=kOutput, calls=%fused_computation.10 | convolution fusion | flops 805830656 | bytes 1835016 | tf_op jit(solution)/shard_map/dot_general | solution.py:80
  155.1 14.2 %all-reduce = (f32[]{:T(128)}, f32[]{:T(128)}) all-reduce(f32[]{:T(128)} %get-tuple-element.31, f32[]{:T(128)} %get-tuple-element.33), channel_id=1, replica_groups=mesh['fs'=4,'tp'=8] {'tp'}, use_global_device_ids=true, to_apply=%region_4.0 | all-reduce | flops 2 | bytes 16 | tf_op jit(solution)/shard_map/psum | solution.py:83
  169.4 9.5 %all-reduce.2 = (f32[]{:T(128)}, f32[]{:T(128)}) all-reduce(f32[]{:T(128)} %get-tuple-element.10, f32[]{:T(128)} %get-tuple-element.11), channel_id=1, replica_groups=mesh['fs'=4,'tp'=8] {'fs'}, use_global_device_ids=true, to_apply=%region_5.0 | all-reduce | flops 2 | bytes 16 | tf_op jit(solution)/shard_map/psum | solution.py:82
  179.6 3.1 %fusion.21 = (bf16[512,512]{1,0:T(8,128)(2,1)}, f32[512,512]{1,0:T(8,128)}, f32[512,512]{1,0:T(8,128)}) fusion(f32[512,512]{1,0:T(8,128)} %param.22, f32[512,512]{1,0:T(8,128)S(1)} %get-tuple-element.32, f32[]{:T(128)S(6)} %rsqrt.6), kind=kLoop, calls=%fused_computation.41 | loop fusion | flops 1048576 | bytes 4718596 | tf_op jit(solution)/shard_map/convert_element_type | solution.py:90
  182.7 0.0 all-gather.3.cloned.1.call-update
  182.7 0.0 all-gather.5.cloned.1.call-start
  182.7 1.6 copy.24
  185.0 3.1 %fusion.20 = (bf16[512,512]{1,0:T(8,128)(2,1)}, f32[512,512]{1,0:T(8,128)}, f32[512,512]{1,0:T(8,128)}) fusion(f32[512,512]{1,0:T(8,128)} %param.23, f32[512,512]{0,1:T(8,128)S(1)} %copy.24, f32[]{:T(128)S(6)} %rsqrt.7), kind=kLoop, calls=%fused_computation.40 | loop fusion | flops 1048576 | bytes 4718596 | tf_op jit(solution)/shard_map/convert_element_type | solution.py:91
  188.2 26.5 %all-gather.3.cloned.1.call-done = bf16[2048,512]{1,0:T(8,128)(2,1)} async-done(((bf16[512,512]{1,0:T(8,128)(2,1)}), bf16[2048,512]{1,0:T(8,128)(2,1)}) %all-gather.3.cloned.1.call-update) | async-done | bytes 2097168 | tf_op jit(solution)/shard_map/all_gather | solution.py:90
  214.7 37.3 %all-gather.5.cloned.1.call-done = bf16[512,2048]{1,0:T(8,128)(2,1)} async-done(((bf16[512,512]{1,0:T(8,128)(2,1)}), bf16[512,2048]{1,0:T(8,128)(2,1)}) %all-gather.5.cloned.1.call-update) | async-done | bytes 2097168 | tf_op jit(solution)/shard_map/all_gather | solution.py:91
  252.0 3.2 %copy.29 = bf16[2048,512]{1,0:T(8,128)(2,1)} copy(bf16[2048,512]{1,0:T(8,128)(2,1)} %all-gather.3.cloned.1.call-done) | data formatting | bytes 4194304
  255.2 1.3 copy.30
  (24 shorter events, 0.1 us)
Async XLA Ops:
  7.2 86.5 %copy-start = (bf16[1536,512]{1,0:T(8,128)(2,1)S(1)}, bf16[1536,512]{1,0:T(8,128)(2,1)}, u32[]{:S(2)}) copy-start(bf16[1536,512]{1,0:T(8,128)(2,1)} %param.19) | copy-start | bytes 4718596
  7.2 3.7 %copy-start.9 = (f32[256]{0:T(256)S(1)}, f32[256]{0:T(256)}, u32[]{:S(2)}) copy-start(f32[256]{0:T(256)} %param.17) | copy-start | bytes 3076
  7.2 3.7 %copy-start.11 = (bf16[1536,256]{1,0:T(8,128)(2,1)S(1)}, bf16[1536,256]{1,0:T(8,128)(2,1)}, u32[]{:S(2)}) copy-start(bf16[1536,256]{1,0:T(8,128)(2,1)} %param.16) | copy-start | bytes 2359300
  7.2 3.7 %copy-start.10 = (bf16[1536,256]{1,0:T(8,128)(2,1)S(1)}, bf16[1536,256]{1,0:T(8,128)(2,1)}, u32[]{:S(2)}) copy-start(bf16[1536,256]{1,0:T(8,128)(2,1)} %param.15) | copy-start | bytes 2359300
  7.2 86.4 %all-reduce.5.cloned.1.call-start = ((), (), s32[]{:S(2)}) async-start(), calls=%async_computation.4 | async-start | bytes 6291456 | tf_op jit(solution)/shard_map/psum | solution.py:67
  13.9 114.1 %reduce-scatter.2.cloned.1.call-start = ((), (), s32[]{:S(2)}) async-start(), calls=%async_computation.1 | async-start | bytes 1310720 | tf_op jit(solution)/shard_map/reduce_scatter | solution.py:70
  93.7 2.1 copy-start.3
  95.8 1.4 copy-start.1
  95.8 1.9 copy-start.2
  98.9 29.2 %copy-start.5 = (f32[64,512]{1,0:T(8,128)S(1)}, f32[64,512]{1,0:T(8,128)}, u32[]{:S(2)}) copy-start(f32[64,512]{1,0:T(8,128)} %param.27) | copy-start | bytes 393220
  98.9 29.2 %copy-start.6 = (f32[64,512]{1,0:T(8,128)S(1)}, f32[64,512]{1,0:T(8,128)}, u32[]{:S(2)}) copy-start(f32[64,512]{1,0:T(8,128)} %param.26) | copy-start | bytes 393220
  98.9 29.1 %copy-start.7 = (f32[64,512]{1,0:T(8,128)S(1)}, f32[64,512]{1,0:T(8,128)}, u32[]{:S(2)}) copy-start(f32[64,512]{1,0:T(8,128)} %param.25) | copy-start | bytes 393220
  98.9 29.1 %copy-start.8 = (f32[64,512]{1,0:T(8,128)S(1)}, f32[64,512]{1,0:T(8,128)}, u32[]{:S(2)}) copy-start(f32[64,512]{1,0:T(8,128)} %param.24) | copy-start | bytes 393220
  100.0 114.7 %all-gather.3.cloned.1.call-start = ((), (), s32[]{:S(2)}) async-start(), calls=%async_computation.2 | async-start | bytes 2621440 | tf_op jit(solution)/shard_map/all_gather | solution.py:90
  182.7 69.3 %all-gather.5.cloned.1.call-start = ((), (), s32[]{:S(2)}) async-start(), calls=%async_computation.3 | async-start | bytes 2621440 | tf_op jit(solution)/shard_map/all_gather | solution.py:91
  252.0 3.2 %copy-start.4 = (bf16[512,2048]{1,0:T(8,128)(2,1)S(1)}, bf16[512,2048]{1,0:T(8,128)(2,1)}, u32[]{:S(2)}) copy-start(bf16[512,2048]{1,0:T(8,128)(2,1)} %all-gather.5.cloned.1.call-done) | copy-start | bytes 6291460
Sparse Core Ops, SparseCore 0:
  14.0 79.5 all-reduce.4
  100.1 27.8 reduce-scatter.1
  182.8 31.8 all-gather.2
  216.9 35.0 all-gather.4
